TPU v7x, 32 devices: a whole 2x2x4 slice. The times are simulated.
32 devices in a mesh: sp: 8 (over z, y), dp: 4 (over x, core).
Axes of the slice: x: 2, y: 2, z: 4, core: 2. Of those that a mesh axis runs over, the one named last changes fastest.
Arguments:
- tokens: bfloat16 [4, 2048, 2048], P('dp', 'sp'), may hold values from -6 to 6
- w_query: bfloat16 [2048, 2048], P('dp', 'sp'), may hold values from -0.125 to 0.125
- w_key: bfloat16 [2048, 1024], P('dp', 'sp'), may hold values from -0.125 to 0.125
- w_value: bfloat16 [2048, 1024], P('dp', 'sp'), may hold values from -0.125 to 0.125
- w_out: bfloat16 [2048, 2048], P('dp', 'sp'), may hold values from -0.25 to 0.25
- qk_gain: float32 [2, 128], replicated, may hold values from 0.9 to 24
Outputs:
- mixed_out: bfloat16 [4, 2048, 2048], P('dp', 'sp')
All inputs are finite; a program needn't handle non-finite values.
Results may differ from a plain program's by a relative error of at most 0.006.
The roundings to bfloat16 on the way count: a program that leaves them out, or rounds other values in their place, can miss the bound.
Values may be sent and summed in bfloat16 or wider, within the bound.
A program may use at most 64 MiB of HBM per device.

v0:
```python
import math

import jax
import jax.numpy as jnp
import numpy as np
from jax import lax
from jax.sharding import PartitionSpec as P

HQ = 16
KV = 8
HD = 128
GRID_W = 64


ROPE_BASE = 10000.0
EPS = 1e-06


def angles(positions):
    quarter = jnp.arange(0, HD // 2, 2, dtype=jnp.float32)
    inv_freq = ROPE_BASE ** (-quarter / (HD // 2))
    row_pos = (positions // GRID_W).astype(jnp.float32)
    col_pos = (positions % GRID_W).astype(jnp.float32)
    angle_table = jnp.concatenate(
        [row_pos[:, None] * inv_freq, col_pos[:, None] * inv_freq], axis=1
    )
    return (jnp.cos(angle_table), jnp.sin(angle_table))


def prepare(raw_proj, gain_row, cosine, sine_table):
    normed = (
        raw_proj * lax.rsqrt(jnp.mean(raw_proj * raw_proj, axis=-1, keepdims=True) + EPS) * gain_row
    )
    pair_view = normed.reshape(raw_proj.shape[:-1] + (HD // 2, 2))
    first_half = pair_view[..., 0]
    second = pair_view[..., 1]
    cos_b = cosine[:, None, :]
    sin_b = sine_table[:, None, :]
    turned = jnp.stack(
        [first_half * cos_b - second * sin_b, first_half * sin_b + second * cos_b], axis=-1
    )
    return turned.reshape(raw_proj.shape).astype(jnp.bfloat16)


def attend_head(query_rows, key_rows, value_rows):
    seq_len = query_rows.shape[0]
    block_len = math.gcd(seq_len, 512)
    blocks = query_rows.reshape(seq_len // block_len, block_len, HD)

    def one_block(row_block):
        scores = jnp.dot(row_block, key_rows.T, preferred_element_type=jnp.float32) * HD ** (-0.5)
        top_score = jnp.max(scores, axis=1, keepdims=True)
        weights = jnp.exp(scores - top_score)
        row_total = jnp.sum(weights, axis=1, keepdims=True)
        probs_bf = (weights / row_total).astype(jnp.bfloat16)
        return jnp.dot(probs_bf, value_rows, preferred_element_type=jnp.float32).astype(
            jnp.bfloat16
        )

    return lax.map(one_block, blocks).reshape(seq_len, HD)


def project(own_rows, weight):
    col_full = lax.all_gather(weight, "sp", axis=1, tiled=True)
    return jnp.dot(
        own_rows,
        lax.all_gather(col_full, "dp", axis=0, tiled=True),
        preferred_element_type=jnp.float32,
    )


def on_device(tokens, w_query, w_key, w_value, w_out, qk_gain):
    own_rows = tokens[0]
    n_seqdev = lax.axis_size("sp")
    tok_local = own_rows.shape[0]
    positions = lax.axis_index("sp") * tok_local + jnp.arange(tok_local, dtype=jnp.int32)
    cosine, sine_table = angles(positions)
    heads_dev = HQ // n_seqdev
    group_size = HQ // KV
    kv_dev = max(1, heads_dev // group_size)
    chosen = (np.arange(n_seqdev) * heads_dev // group_size)[:, None] + np.arange(kv_dev)[None, :]
    chosen = chosen.reshape(-1)
    key_all = prepare(
        project(own_rows, w_key).reshape(tok_local, KV, HD), qk_gain[1], cosine, sine_table
    )
    values = project(own_rows, w_value).astype(jnp.bfloat16).reshape(tok_local, KV, HD)
    key_send = key_all[:, chosen, :].reshape(tok_local, -1)
    value_send = values[:, chosen, :].reshape(tok_local, -1)
    raw_proj = project(own_rows, w_query).reshape(tok_local, HQ, HD)
    query_heads = lax.all_to_all(
        prepare(raw_proj, qk_gain[0], cosine, sine_table).reshape(tok_local, HQ * HD),
        "sp",
        split_axis=1,
        concat_axis=0,
        tiled=True,
    )
    key_heads = lax.all_to_all(key_send, "sp", split_axis=1, concat_axis=0, tiled=True)
    value_heads = lax.all_to_all(value_send, "sp", split_axis=1, concat_axis=0, tiled=True)
    outputs = []
    for head_index in range(heads_dev):
        kv_slot = head_index // group_size if heads_dev >= group_size else 0
        outputs.append(
            attend_head(
                query_heads[:, head_index * HD : (head_index + 1) * HD],
                key_heads[:, kv_slot * HD : (kv_slot + 1) * HD],
                value_heads[:, kv_slot * HD : (kv_slot + 1) * HD],
            )
        )
    mixed_heads = jnp.concatenate(outputs, axis=1)
    token_rows = lax.all_to_all(mixed_heads, "sp", split_axis=0, concat_axis=1, tiled=True)
    return project(token_rows, w_out).astype(jnp.bfloat16)[None]


def solution(mesh):
    in_specs = (
        P("dp", "sp", None),
        P("dp", "sp"),
        P("dp", "sp"),
        P("dp", "sp"),
        P("dp", "sp"),
        P(),
    )
    out_specs = P("dp", "sp", None)
    return jax.shard_map(
        on_device, mesh=mesh, in_specs=in_specs, out_specs=out_specs, check_vma=False
    )
```

profile of v0, /device:TPU:13, one launch (start us, length us, event | category | flops | bytes accessed | tf_op | source)
XLA Modules:
  0.0 412.9 jit_solution(12027826076929534750)
XLA Ops:
  8.8 38.9 %all-gather.17.cloned.1.call-done = bf16[512,1024]{1,0:T(8,128)(2,1)} async-done(((bf16[512,128]{1,0:T(8,128)(2,1)}), bf16[512,1024]{1,0:T(8,128)(2,1)}) %all-gather.17.cloned.1.call-update) | async-done | bytes 1048592 | tf_op jit(solution)/shard_map/all_gather | solution.py:64
  47.8 50.3 %all-gather.9.cloned.1.call-done = bf16[512,2048]{1,0:T(8,128)(2,1)} async-done(((bf16[512,256]{1,0:T(8,128)(2,1)}), bf16[512,2048]{1,0:T(8,128)(2,1)}) %all-gather.9.cloned.1.call-update) | async-done | bytes 2097168 | tf_op jit(solution)/shard_map/all_gather | solution.py:64
  98.2 40.6 %all-gather.13.cloned.1.call-done = bf16[512,1024]{1,0:T(8,128)(2,1)} async-done(((bf16[512,128]{1,0:T(8,128)(2,1)}), bf16[512,1024]{1,0:T(8,128)(2,1)}) %all-gather.13.cloned.1.call-update) | async-done | bytes 1048592 | tf_op jit(solution)/shard_map/all_gather | solution.py:64
  140.0 36.3 %all-gather.19.cloned.1.call-done = bf16[2048,1024]{1,0:T(8,128)(2,1)} async-done(((bf16[512,1024]{1,0:T(8,128)(2,1)}), bf16[2048,1024]{1,0:T(8,128)(2,1)}) %all-gather.19.cloned.1.call-update) | async-done | bytes 4194320 | tf_op jit(solution)/shard_map/all_gather | solution.py:67
  176.3 3.4 fusion.21
  181.4 5.5 %all-to-all-start.2 = ((bf16[256,8,128]{2,0,1:T(8,128)(2,1)}), bf16[256,8,128]{2,0,1:T(8,128)(2,1)}, u32[]{:S(2)}, u32[]{:S(2)}) async-start(bf16[256,8,128]{2,0,1:T(8,128)(2,1)} %bitcast.19), calls=%async_computation.2 | async-start | bytes 1048576 | tf_op jit(solution)/shard_map/all_to_all | solution.py:98
  186.8 49.2 %all-gather.11.cloned.1.call-done = bf16[2048,2048]{1,0:T(8,128)(2,1)} async-done(((bf16[512,2048]{1,0:T(8,128)(2,1)}), bf16[2048,2048]{1,0:T(8,128)(2,1)}) %all-gather.11.cloned.1.call-update) | async-done | bytes 8388624 | tf_op jit(solution)/shard_map/all_gather | solution.py:67
  236.1 12.2 %copy.19 = bf16[2048,2048]{1,0:T(8,128)(2,1)} copy(bf16[2048,2048]{0,1:T(8,128)(2,1)} %bitcast.93) | data formatting | bytes 16777216 | tf_op jit(solution)/shard_map/dot_general | solution.py:65
  248.3 5.8 %multiply_reduce_fusion.2 = (f32[256,16]{0,1:T(8,128)S(1)}, f32[256,16,128]{0,2,1:T(8,128)S(1)}) fusion(bf16[16,128,2048]{2,1,0:T(8,128)(2,1)} %bitcast.94, bf16[1,256,2048]{2,1,0:T(8,128)(2,1)S(1)} %copy-done), kind=kOutput, calls=%fused_computation.31 | convolution fusion | flops 2148528128 | bytes 11550720 | tf_op jit(solution)/shard_map/dot_general | solution.py:65
  255.9 2.5 reshape.165
  258.4 2.9 subtract_convert_fusion
  261.3 2.4 pad_maximum_fusion
  264.9 5.5 %all-to-all-start = ((bf16[256,8,256]{0,2,1:T(8,128)(2,1)}), bf16[256,8,256]{0,2,1:T(8,128)(2,1)S(1)}, u32[]{:S(2)}, u32[]{:S(2)}) async-start(bf16[256,8,256]{0,2,1:T(8,128)(2,1)} %convert_element_type.44), calls=%async_computation | async-start | bytes 2097152 | tf_op jit(solution)/shard_map/all_to_all | solution.py:90
  271.9 6.5 %copy.21 = bf16[1024,2048]{1,0:T(8,128)(2,1)} copy(bf16[1024,2048]{0,1:T(8,128)(2,1)} %bitcast.96) | data formatting | bytes 8388608 | tf_op jit(solution)/shard_map/dot_general | solution.py:65
  278.5 3.5 multiply_reduce_fusion.3
  284.9 16.2 %all-to-all-done = bf16[256,8,256]{0,2,1:T(8,128)(2,1)S(1)} async-done(((bf16[256,8,256]{0,2,1:T(8,128)(2,1)}), bf16[256,8,256]{0,2,1:T(8,128)(2,1)S(1)}, u32[]{:S(2)}, u32[]{:S(2)}) %all-to-all-start) | async-done | bytes 1048608 | tf_op jit(solution)/shard_map/all_to_all | solution.py:90
  301.0 6.3 %all-to-all-start.1 = ((bf16[256,8,128]{2,0,1:T(8,128)(2,1)}), bf16[256,8,128]{2,0,1:T(8,128)(2,1)S(1)}, u32[]{:S(2)}, u32[]{:S(2)}) async-start(bf16[256,8,128]{2,0,1:T(8,128)(2,1)} %bitcast.16), calls=%async_computation.1 | async-start | bytes 1048576 | tf_op jit(solution)/shard_map/all_to_all | solution.py:97
  307.4 31.4 %all-gather.21.cloned.1.call-done = bf16[512,2048]{1,0:T(8,128)(2,1)} async-done(((bf16[512,256]{1,0:T(8,128)(2,1)}), bf16[512,2048]{1,0:T(8,128)(2,1)}) %all-gather.21.cloned.1.call-update) | async-done | bytes 2097168 | tf_op jit(solution)/shard_map/all_gather | solution.py:64
  339.5 15.0 %while.21 = (s32[]{:T(128)}, bf16[4,512,128]{2,1,0:T(8,128)(2,1)S(1)}, bf16[4,512,128]{2,1,0:T(8,128)(2,1)S(1)}, bf16[2048,128]{1,0:T(8,128)(2,1)S(1)}, bf16[2048,128]{1,0:T(8,128)(2,1)}, /*index=5*/s32[]{:T(128)}) while((s32[]{:T(128)}, bf16[4,512,128]{2,1,0:T(8,128)(2,1)S(1)}, bf16[4,512,128]{2,1,0:T(8,128)(2,1)S(1)}, ...), condition=%wide.region_9.10_spmd, body=%wide.region_6.9_spmd.sunk | while | flops 546372608 | bytes 13903957 | solution.py:60
  348.6 2.2 fusion.57
  352.4 2.1 fusion.57
  354.6 14.9 %while.20 = (s32[]{:T(128)}, bf16[4,512,128]{2,1,0:T(8,128)(2,1)S(1)}, bf16[4,512,128]{2,1,0:T(8,128)(2,1)S(1)}, bf16[2048,128]{1,0:T(8,128)(2,1)S(1)}, bf16[2048,128]{1,0:T(8,128)(2,1)}, /*index=5*/s32[]{:T(128)}) while((s32[]{:T(128)}, bf16[4,512,128]{2,1,0:T(8,128)(2,1)S(1)}, bf16[4,512,128]{2,1,0:T(8,128)(2,1)S(1)}, ...), condition=%wide.region_5.6_spmd, body=%wide.region_2.5_spmd.sunk | while | flops 546372608 | bytes 13903957 | solution.py:60
  369.7 28.1 %all_to_all.64 = bf16[8,256,256]{2,1,0:T(8,128)(2,1)S(1)} all-to-all(bf16[8,256,256]{2,1,0:T(8,128)(2,1)S(1)} %pad_maximum_fusion.1), channel_id=1, replica_groups=mesh['sp'=8,'dp'=4] {'sp'}, dimensions={0} | all-to-all | bytes 2097152 | tf_op jit(solution)/shard_map/all_to_all | solution.py:110
  399.2 6.8 %fusion.20 = bf16[1,256,2048]{2,1,0:T(8,128)(2,1)} fusion(bf16[256,2048]{0,1:T(8,128)(2,1)S(1)} %bitcast.95, bf16[2048,2048]{1,0:T(8,128)(2,1)} %all-gather.23.cloned.1.call-done), kind=kOutput, calls=%fused_computation.29 | convolution fusion | flops 2148007936 | bytes 10485760 | tf_op jit(solution)/shard_map/dot_general | solution.py:65
  (73 shorter events, 40.2 us)
Async XLA Ops:
  6.5 169.8 %copy-start = (bf16[1,256,2048]{2,1,0:T(8,128)(2,1)S(1)}, bf16[1,256,2048]{2,1,0:T(8,128)(2,1)}, u32[]{:S(2)}) copy-start(bf16[1,256,2048]{2,1,0:T(8,128)(2,1)} %param.13) | copy-start | bytes 3145732
  6.5 133.1 %copy-start.2 = (f32[2,128]{1,0:T(2,128)S(1)}, f32[2,128]{1,0:T(2,128)}, u32[]{:S(2)}) copy-start(f32[2,128]{1,0:T(2,128)} %param.18) | copy-start | bytes 3076
  6.5 41.2 %all-gather.17.cloned.1.call-start = ((), (), s32[]{:S(2)}) async-start(), calls=%async_computation.8 | async-start | bytes 1179648 | tf_op jit(solution)/shard_map/all_gather | solution.py:64
  7.3 90.9 %all-gather.9.cloned.1.call-start = ((), (), s32[]{:S(2)}) async-start(), calls=%async_computation.4 | async-start | bytes 2359296 | tf_op jit(solution)/shard_map/all_gather | solution.py:64
  8.0 130.8 %all-gather.13.cloned.1.call-start = ((), (), s32[]{:S(2)}) async-start(), calls=%async_computation.6 | async-start | bytes 1179648 | tf_op jit(solution)/shard_map/all_gather | solution.py:64
  8.7 167.6 %all-gather.19.cloned.1.call-start = ((), (), s32[]{:S(2)}) async-start(), calls=%async_computation.9 | async-start | bytes 5242880 | tf_op jit(solution)/shard_map/all_gather | solution.py:67
  47.8 188.3 %all-gather.11.cloned.1.call-start = ((), (), s32[]{:S(2)}) async-start(), calls=%async_computation.5 | async-start | bytes 10485760 | tf_op jit(solution)/shard_map/all_gather | solution.py:67
  98.2 173.8 %all-gather.15.cloned.1.call-start = ((), (), s32[]{:S(2)}) async-start(), calls=%async_computation.7 | async-start | bytes 5242880 | tf_op jit(solution)/shard_map/all_gather | solution.py:67
  138.9 199.9 %all-gather.21.cloned.1.call-start = ((), (), s32[]{:S(2)}) async-start(), calls=%async_computation.10 | async-start | bytes 2359296 | tf_op jit(solution)/shard_map/all_gather | solution.py:64
  181.4 83.6 %all-to-all-start.2 = ((bf16[256,8,128]{2,0,1:T(8,128)(2,1)}), bf16[256,8,128]{2,0,1:T(8,128)(2,1)}, u32[]{:S(2)}, u32[]{:S(2)}) async-start(bf16[256,8,128]{2,0,1:T(8,128)(2,1)} %bitcast.19), calls=%async_computation.2 | async-start | bytes 1048576 | tf_op jit(solution)/shard_map/all_to_all | solution.py:98
  264.9 36.1 %all-to-all-start = ((bf16[256,8,256]{0,2,1:T(8,128)(2,1)}), bf16[256,8,256]{0,2,1:T(8,128)(2,1)S(1)}, u32[]{:S(2)}, u32[]{:S(2)}) async-start(bf16[256,8,256]{0,2,1:T(8,128)(2,1)} %convert_element_type.44), calls=%async_computation | async-start | bytes 2097152 | tf_op jit(solution)/shard_map/all_to_all | solution.py:90
  301.0 38.4 %all-to-all-start.1 = ((bf16[256,8,128]{2,0,1:T(8,128)(2,1)}), bf16[256,8,128]{2,0,1:T(8,128)(2,1)S(1)}, u32[]{:S(2)}, u32[]{:S(2)}) async-start(bf16[256,8,128]{2,0,1:T(8,128)(2,1)} %bitcast.16), calls=%async_computation.1 | async-start | bytes 1048576 | tf_op jit(solution)/shard_map/all_to_all | solution.py:97
  307.4 91.9 %all-gather.23.cloned.1.call-start = ((), (), s32[]{:S(2)}) async-start(), calls=%async_computation.11 | async-start | bytes 10485760 | tf_op jit(solution)/shard_map/all_gather | solution.py:67
  399.2 6.8 %copy-start.1 = (bf16[1,256,2048]{2,1,0:T(8,128)(2,1)S(1)}, bf16[1,256,2048]{2,1,0:T(8,128)(2,1)}, u32[]{:S(2)}) copy-start(bf16[1,256,2048]{2,1,0:T(8,128)(2,1)} %param.13) | copy-start | bytes 3145732
Sparse Core Ops, SparseCore 0:
  9.4 38.3 all-gather.16
  49.8 48.3 all-gather.8
  100.2 38.5 all-gather.12
  140.2 36.0 all-gather.18
  177.7 58.2 all-gather.10
  237.5 34.4 all-gather.14
  274.0 64.7 all-gather.20
  340.3 58.8 all-gather.22
where the time goes:
time: 418 us; the launch traced here: 413 us
  waiting for transfers between devices  268 us (64%)
  matrix products  42.8 us (10%)
  blocking collectives  28.1 us (7%)
  local copies, waits for them, and re-layouts  27.8 us (7%)
  starting transfers between devices  17.5 us (4%)
  other arithmetic  14.5 us (3%)
  between operations  13.7 us (3%)
    all_gather x4, waiting for transfers between devices, project(): col_full = lax.all_gather(weight, 'sp', axis=1, tiled=True)  161 us
    all_gather x4, waiting for transfers between devices, project(): lax.all_gather(col_full, 'dp', axis=0, tiled=True)  88.1 us
    all_to_all x1, blocking collectives, on_device(): lax.all_to_all(mixed_heads, 'sp', split_axis=0, concat_axis=1, tiled=True)  28.1 us
    dot_general x4, matrix products, project(): jnp.dot(own_rows, lax.all_gather(col_full, 'dp', axis=0, tiled=True), pre...  19.6 us
    dot_general x2, local copies, waits for them, and re-layouts, project(): jnp.dot(own_rows, lax.all_gather(col_full, 'dp', axis=0, tiled=True), pre...  18.8 us
    dot_general x8, matrix products, one_block(): jnp.dot(probs_bf, value_rows, preferred_element_type=jnp.float32)  16.9 us
    all_to_all x1, waiting for transfers between devices, on_device(): lax.all_to_all(prepare(raw_proj, qk_gain[0], cosine, sine_table).reshape(...  16.2 us
  transfers between devices with their start and end apart: 11, of which 9 were waited for; matrix products, arithmetic and copies ran while one was open for 19% of the time, Pallas kernels for 0%

commit v1 on v0

v1 whole, which is shorter than its diff:
```python
import functools

import jax
import jax.numpy as jnp
from jax import lax
from jax.experimental import pallas as pl
from jax.experimental.pallas import tpu as pltpu
from jax.sharding import PartitionSpec as P

HQ = 16
KV = 8
HD = 128
GRID_W = 64
ROPE_BASE = 10000.0
EPS = 1e-06
LOG2E = 1.4426950408889634
VMEM_CAP = 60 * 1024 * 1024


def rope_tables(seq_len):
    quarter = jnp.arange(0, HD // 2, 2, dtype=jnp.float32)
    inv_freq = jnp.repeat(ROPE_BASE ** (-quarter / (HD // 2)), 2)
    rows = jnp.arange(seq_len // GRID_W, dtype=jnp.int32).astype(jnp.float32)
    cols = jnp.arange(GRID_W, dtype=jnp.int32).astype(jnp.float32)
    row_angle = rows[:, None] * inv_freq
    col_angle = cols[:, None] * inv_freq
    sign = jnp.where(jnp.arange(HD // 2) % 2 == 0, -1.0, 1.0).astype(jnp.float32)

    def table(fn):
        by_row = jnp.broadcast_to(fn(row_angle)[:, None, :], (seq_len // GRID_W, GRID_W, HD // 2))
        by_col = jnp.broadcast_to(fn(col_angle)[None, :, :], (seq_len // GRID_W, GRID_W, HD // 2))
        return jnp.concatenate([by_row, by_col], axis=2).reshape(seq_len, HD)

    return table(jnp.cos), table(lambda a: jnp.sin(a) * sign)


def attention_kernel(
    nb, tb, tq, hq, hk, x_ref, w_ref, cos_ref, sin_ref, gain_ref, o_ref, q_s, k_s, v_s
):
    i = pl.program_id(0)

    @pl.when(i < nb)
    def _():
        raw = jnp.dot(x_ref[...], w_ref[...], preferred_element_type=jnp.float32)
        cosine = cos_ref[...]
        sine = sin_ref[...]
        even = lax.broadcasted_iota(jnp.int32, (tb, HD), 1) % 2 == 0
        rows = pl.ds(pl.multiple_of(i * tb, tb), tb)
        for h in range(hq + hk):
            r = raw[:, h * HD : (h + 1) * HD]
            gain = gain_ref[0:1, :] if h < hq else gain_ref[1:2, :]
            n = r * lax.rsqrt(jnp.mean(r * r, axis=-1, keepdims=True) + EPS) * gain
            swapped = jnp.where(even, pltpu.roll(n, HD - 1, 1), pltpu.roll(n, 1, 1))
            turned = (n * cosine + swapped * sine).astype(jnp.bfloat16)
            if h < hq:
                q_s[h, rows, :] = turned
            else:
                k_s[h - hq, rows, :] = turned
        for h in range(hk):
            v_s[h, rows, :] = raw[:, (hq + hk + h) * HD : (hq + hk + h + 1) * HD].astype(
                jnp.bfloat16
            )

    @pl.when(i >= nb)
    def _():
        rows = pl.ds(pl.multiple_of((i - nb) * tq, tq), tq)
        c = HD ** (-0.5) * LOG2E
        for h in range(hq):
            g = h * hk // hq
            s = lax.dot_general(
                q_s[h, rows, :],
                k_s[g],
                (((1,), (1,)), ((), ())),
                preferred_element_type=jnp.float32,
            )
            p = jnp.exp2((s - jnp.max(s, axis=1, keepdims=True)) * c)
            inv = 1.0 / jnp.sum(p, axis=1, keepdims=True)
            probs = (p * inv).astype(jnp.bfloat16)
            o_ref[:, h * HD : (h + 1) * HD] = jnp.dot(
                probs, v_s[g], preferred_element_type=jnp.float32
            ).astype(jnp.bfloat16)


def attend(seq_rows, weights, cosine, sine, gain, hq, hk):
    seq_len, width = seq_rows.shape
    tb = min(512, seq_len)
    tq = min(256, seq_len)
    nb, nq = seq_len // tb, seq_len // tq
    block = lambda i: (jnp.minimum(i, nb - 1), 0)
    whole = lambda i: (0, 0)
    return pl.pallas_call(
        functools.partial(attention_kernel, nb, tb, tq, hq, hk),
        grid=(nb + nq,),
        out_shape=jax.ShapeDtypeStruct((seq_len, hq * HD), jnp.bfloat16),
        in_specs=[
            pl.BlockSpec((tb, width), block),
            pl.BlockSpec(weights.shape, whole),
            pl.BlockSpec((tb, HD), block),
            pl.BlockSpec((tb, HD), block),
            pl.BlockSpec(gain.shape, whole),
        ],
        out_specs=pl.BlockSpec((tq, hq * HD), lambda i: (jnp.maximum(i - nb, 0), 0)),
        scratch_shapes=[
            pltpu.VMEM((hq, seq_len, HD), jnp.bfloat16),
            pltpu.VMEM((hk, seq_len, HD), jnp.bfloat16),
            pltpu.VMEM((hk, seq_len, HD), jnp.bfloat16),
        ],
        compiler_params=pltpu.CompilerParams(vmem_limit_bytes=VMEM_CAP),
        cost_estimate=pl.CostEstimate(
            flops=2 * seq_len * width * weights.shape[1] + 4 * hq * seq_len * seq_len * HD,
            bytes_accessed=2 * (seq_rows.size + weights.size),
            transcendentals=hq * seq_len * seq_len,
        ),
    )(seq_rows, weights, cosine, sine, gain)


def mix_kernel(a_ref, w_ref, o_ref):
    n_src, tok, feat = a_ref.shape
    per = w_ref.shape[2] // feat
    total = None
    for s in range(n_src):
        term = jnp.dot(
            a_ref[s],
            w_ref[s // per, 0, (s % per) * feat : (s % per + 1) * feat, :],
            preferred_element_type=jnp.float32,
        )
        total = term if total is None else total + term
    o_ref[...] = total.astype(o_ref.dtype)


def mix(attended, w_all):
    n_src, tok, feat = attended.shape
    n_dp, n_sp, depth, cols = w_all.shape
    return pl.pallas_call(
        mix_kernel,
        grid=(n_sp,),
        out_shape=jax.ShapeDtypeStruct((tok, n_sp * cols), jnp.bfloat16),
        in_specs=[
            pl.BlockSpec(attended.shape, lambda s: (0, 0, 0)),
            pl.BlockSpec((n_dp, 1, depth, cols), lambda s: (0, s, 0, 0)),
        ],
        out_specs=pl.BlockSpec((tok, cols), lambda s: (0, s)),
        compiler_params=pltpu.CompilerParams(vmem_limit_bytes=VMEM_CAP),
        cost_estimate=pl.CostEstimate(
            flops=2 * tok * w_all.size, bytes_accessed=2 * w_all.size, transcendentals=0
        ),
    )(attended, w_all)


def head_columns(weight, n_sp):
    local = weight.shape[1]
    if local >= HD:
        return weight
    group = HD // local
    groups = [list(range(g, g + group)) for g in range(0, n_sp, group)]
    return lax.all_gather(weight, "sp", axis=1, tiled=True, axis_index_groups=groups)


def on_device(tokens, w_query, w_key, w_value, w_out, qk_gain):
    n_sp = lax.axis_size("sp")
    n_dp = lax.axis_size("dp")
    own_rows = tokens[0]
    tok = own_rows.shape[0]
    seq_len = tok * n_sp
    hq = HQ // n_sp
    hk = max(1, KV // n_sp)
    cosine, sine = rope_tables(seq_len)
    w_local = jnp.concatenate(
        [w_query, head_columns(w_key, n_sp), head_columns(w_value, n_sp)], axis=1
    )
    weights = lax.all_gather(w_local, "dp", axis=0, tiled=True)
    seq_rows = lax.all_gather(own_rows, "sp", axis=0, tiled=True)
    w_all = lax.all_gather(w_out, ("dp", "sp"), axis=0, tiled=False)
    w_all = w_all.reshape((n_dp, n_sp) + w_out.shape)
    attended = attend(seq_rows, weights, cosine, sine, qk_gain, hq, hk)
    blocks = lax.all_to_all(
        attended.reshape(n_sp, tok, hq * HD), "sp", split_axis=0, concat_axis=0, tiled=True
    )
    return mix(blocks, w_all)[None]


def solution(mesh):
    in_specs = (
        P("dp", "sp", None),
        P("dp", "sp"),
        P("dp", "sp"),
        P("dp", "sp"),
        P("dp", "sp"),
        P(),
    )
    return jax.shard_map(
        on_device, mesh=mesh, in_specs=in_specs, out_specs=P("dp", "sp", None), check_vma=False
    )
```

time: 418 us -> 267 us (0.64)
  waiting for transfers between devices: 268 us -> 199 us
  matrix products: 42.8 us -> 0 us
  Pallas kernels: 0 us -> 39.7 us
  blocking collectives: 28.1 us -> 0 us
  local copies, waits for them, and re-layouts: 27.8 us -> 1.61 us
  starting transfers between devices: 17.5 us -> 6.38 us
  other arithmetic: 14.5 us -> 4.93 us
    all_gather x8 -> x3, waiting for transfers between devices: 249 us -> 197 us  [the longest x1 123 us: on_device(): seq_rows = lax.all_gather(own_rows, 'sp', axis=0, tiled=True)]
    dot_general x20 -> x0, matrix products: 42.8 us -> none  [the longest x4 19.6 us: project(): jnp.dot(own_rows, lax.all_gather(col_full, 'dp', axis=0, tiled=True), pre...]
    pallas_call x0 -> x2, Pallas kernels: none -> 39.7 us  [the longest x1 31.1 us: attend(): pl.pallas_call(functools.partial(attention_kernel, nb, tb, tq, hq, hk), g...]
    all_to_all x1 -> x0, blocking collectives: 28.1 us -> none  [on_device(): lax.all_to_all(mixed_heads, 'sp', split_axis=0, concat_axis=1, tiled=True)]
    dot_general x2 -> x0, local copies, waits for them, and re-layouts: 18.8 us -> none  [project(): jnp.dot(own_rows, lax.all_gather(col_full, 'dp', axis=0, tiled=True), pre...]
    all_to_all x3 -> x1, waiting for transfers between devices: 16.2 us -> 0.01 us  [on_device(): lax.all_to_all(attended.reshape(n_sp, tok, hq * HD), 'sp', split_axis=0,...]
    all_to_all x3 -> x1, starting transfers between devices: 17.3 us -> 6.3 us  [on_device(): lax.all_to_all(attended.reshape(n_sp, tok, hq * HD), 'sp', split_axis=0,...]
    reduce_sum x8 -> x0, other arithmetic: 6.59 us -> none  [one_block(): row_total = jnp.sum(weights, axis=1, keepdims=True)]
  transfers between devices with their start and end apart: 11 -> 4, of which waited for: 9 -> 3; matrix products, arithmetic and copies ran while one was open for 19% -> 1% of each run, Pallas kernels for 0% -> 12%
where the time goes in v1:
time: 267 us; the launch traced here: 265 us
  waiting for transfers between devices  199 us (75%)
  Pallas kernels  39.7 us (15%)
  between operations  13.2 us (5%)
  starting transfers between devices  6.38 us (2%)
  other arithmetic  4.93 us (2%)
    all_gather x1, waiting for transfers between devices, on_device(): seq_rows = lax.all_gather(own_rows, 'sp', axis=0, tiled=True)  123 us
    all_gather x1, waiting for transfers between devices, on_device(): w_all = lax.all_gather(w_out, ('dp', 'sp'), axis=0, tiled=False)  55 us
    pallas_call x1, Pallas kernels, attend(): pl.pallas_call(functools.partial(attention_kernel, nb, tb, tq, hq, hk), g...  31.1 us
    all_gather x1, waiting for transfers between devices, on_device(): weights = lax.all_gather(w_local, 'dp', axis=0, tiled=True)  19.4 us
    pallas_call x1, Pallas kernels, mix(): pl.pallas_call(mix_kernel, grid=(n_sp,), out_shape=jax.ShapeDtypeStruct((...  8.65 us
    all_to_all x1, starting transfers between devices, on_device(): lax.all_to_all(attended.reshape(n_sp, tok, hq * HD), 'sp', split_axis=0,...  6.3 us
  transfers between devices with their start and end apart: 4, of which 3 were waited for; matrix products, arithmetic and copies ran while one was open for 1% of the time, Pallas kernels for 12%

profile of v1, /device:TPU:13, one launch (start us, length us, event | category | flops | bytes accessed | tf_op | source)
XLA Modules:
  0.0 264.6 jit_solution(17273801167778473923)
XLA Ops:
  6.5 1.9 pad_maximum_fusion.2
  8.5 0.0 all-gather.6.cloned.1.call-update
  8.5 0.0 all-gather.8.cloned.1.call-start
  8.6 0.7 all-gather.8.cloned.1.call-update
  9.3 0.0 all-gather.10.cloned.1.call-start
  9.3 0.7 all-gather.10.cloned.1.call-update
  10.0 0.1 broadcast_in_dim.48
  10.1 0.1 mul.99
  10.2 0.1 fusion.1
  10.4 0.2 fusion
  10.6 0.1 broadcast_in_dim.50
  10.7 0.1 broadcast_in_dim.49
  10.8 1.3 pad_maximum_fusion
  12.1 0.1 broadcast_in_dim.54
  12.2 0.1 broadcast_in_dim.53
  12.3 1.3 pad_maximum_fusion.1
  13.6 19.4 %all-gather.6.cloned.1.call-done.w_ref = bf16[2048,512]{1,0:T(8,128)(2,1)} async-done(((bf16[512,512]{1,0:T(8,128)(2,1)}), bf16[2048,512]{1,0:T(8,128)(2,1)}) %all-gather.6.cloned.1.call-update) | async-done | bytes 2097168 | tf_op jit(solution)/shard_map/all_gather | solution.py:171
  33.0 122.9 %all-gather.8.cloned.1.call-done = bf16[1,2048,2048]{2,1,0:T(8,128)(2,1)} async-done(((bf16[1,256,2048]{2,1,0:T(8,128)(2,1)}), bf16[1,2048,2048]{2,1,0:T(8,128)(2,1)}) %all-gather.8.cloned.1.call-update) | async-done | bytes 8388624 | tf_op jit(solution)/shard_map/all_gather | solution.py:172
  155.9 31.1 %shard_map.64 = bf16[2048,256]{1,0:T(8,128)(2,1)} custom-call(bf16[2048,2048]{1,0:T(8,128)(2,1)} %bitcast.10, bf16[2048,512]{1,0:T(8,128)(2,1)} %all-gather.6.cloned.1.call-done.w_ref, f32[2048,128]{1,0:T(8,128)} %bitcast.7, f32[2048,128]{1,0:T(8,128)} %bitcast.8, f32[2,128]{1,0:T(2,128)} %gain_ref.1), custom_call_target="tpu_custom_call" | custom-call | flops 8589934592 | bytes 10485760 | tf_op jit(solution)/shard_map/pallas_call | solution.py:91
  187.0 6.3 %all-to-all-start = ((bf16[8,256,256]{2,1,0:T(8,128)(2,1)}), bf16[8,256,256]{2,1,0:T(8,128)(2,1)S(1)}, u32[]{:S(2)}, u32[]{:S(2)}) async-start(bf16[8,256,256]{2,1,0:T(8,128)(2,1)} %bitcast.9), calls=%async_computation | async-start | bytes 2097152 | tf_op jit(solution)/shard_map/all_to_all | solution.py:176
  193.3 55.0 %all-gather.10.cloned.1.call-done = bf16[16384,256]{1,0:T(8,128)(2,1)} async-done(((bf16[512,256]{1,0:T(8,128)(2,1)}), bf16[16384,256]{1,0:T(8,128)(2,1)}) %all-gather.10.cloned.1.call-update) | async-done | bytes 8388624 | tf_op jit(solution)/shard_map/all_gather | solution.py:173
  248.3 0.0 all-to-all-done.a_ref
  248.4 1.1 copy-done
  249.4 8.6 %shard_map.65 = bf16[256,2048]{1,0:T(8,128)(2,1)} custom-call(bf16[8,256,256]{2,1,0:T(8,128)(2,1)} %copy-done, bf16[4,8,512,256]{3,2,1,0:T(8,128)(2,1)} %bitcast.6), custom_call_target="tpu_custom_call" | custom-call | flops 2147483648 | bytes 8388608 | tf_op jit(solution)/shard_map/pallas_call | solution.py:134
  (6 shorter events, 0.0 us)
Async XLA Ops:
  6.5 26.5 %all-gather.6.cloned.1.call-start = ((), (), s32[]{:S(2)}) async-start(), calls=%async_computation.1 | async-start | bytes 2621440 | tf_op jit(solution)/shard_map/all_gather | solution.py:171
  8.5 147.4 %all-gather.8.cloned.1.call-start = ((), (), s32[]{:S(2)}) async-start(), calls=%async_computation.2 | async-start | bytes 9437184 | tf_op jit(solution)/shard_map/all_gather | solution.py:172
  9.3 239.1 %all-gather.10.cloned.1.call-start = ((), (), s32[]{:S(2)}) async-start(), calls=%async_computation.3 | async-start | bytes 8650752 | tf_op jit(solution)/shard_map/all_gather | solution.py:173
  187.0 61.3 %all-to-all-start = ((bf16[8,256,256]{2,1,0:T(8,128)(2,1)}), bf16[8,256,256]{2,1,0:T(8,128)(2,1)S(1)}, u32[]{:S(2)}, u32[]{:S(2)}) async-start(bf16[8,256,256]{2,1,0:T(8,128)(2,1)} %bitcast.9), calls=%async_computation | async-start | bytes 2097152 | tf_op jit(solution)/shard_map/all_to_all | solution.py:176
  248.4 1.1 copy-start
Sparse Core Ops, SparseCore 0:
  8.9 24.0 all-gather.5
  35.1 120.7 all-gather.7
  158.9 89.3 all-gather.9

commit v2 on v1

v2 whole, which is shorter than its diff:
```python
import functools

import jax
import jax.numpy as jnp
from jax import lax
from jax.experimental import pallas as pl
from jax.experimental.pallas import tpu as pltpu
from jax.sharding import PartitionSpec as P

HQ = 16
KV = 8
HD = 128
GRID_W = 64
ROPE_BASE = 10000.0
EPS = 1e-06
LOG2E = 1.4426950408889634
VMEM_CAP = 60 * 1024 * 1024


MESH = pl.DeviceIdType.MESH


def rope_tables(seq_len):
    quarter = jnp.arange(0, HD // 2, 2, dtype=jnp.float32)
    inv_freq = jnp.repeat(ROPE_BASE ** (-quarter / (HD // 2)), 2)
    inv_freq = jnp.concatenate([inv_freq, inv_freq])
    count = max(GRID_W, seq_len // GRID_W)
    angle = jnp.arange(count, dtype=jnp.int32).astype(jnp.float32)[:, None] * inv_freq
    sign = jnp.where(jnp.arange(HD) % 2 == 0, -1.0, 1.0).astype(jnp.float32)
    return jnp.cos(angle), jnp.sin(angle) * sign


def layer_kernel(
    n_sp, n_dp, hq, hk,
    tok_ref, wq_ref, wk_ref, wv_ref, wo_ref, cos_ref, sin_ref, gain_ref,
    out_ref,
    x_all, w_all, wo_all, q_s, k_s, v_s, att_s, att_all,
    local_sem, ring_send, ring_recv, w_send, w_recv, wo_send, wo_recv, att_send, att_recv,
):
    tok = tok_ref.shape[0]
    half = n_sp // 2
    me = lax.axis_index("sp")
    dp = lax.axis_index("dp")
    pos = me // 2 + (me % 2) * (n_sp - 1 - 2 * (me // 2))

    def at_pos(p):
        p = lax.rem(p + 2 * n_sp, n_sp)
        return 2 * p + (p // half) * (2 * (n_sp - 1 - p) + 1 - 2 * p)

    q_cols, k_cols = wq_ref.shape[1], wk_ref.shape[1]
    mine = w_all.at[dp]
    loads = [
        (tok_ref, x_all.at[me]),
        (wo_ref, wo_all.at[dp, me]),
        (wq_ref, mine.at[:, 0:q_cols]),
        (wk_ref, mine.at[:, q_cols : q_cols + k_cols]),
        (wv_ref, mine.at[:, q_cols + k_cols : q_cols + 2 * k_cols]),
    ]
    loads = [pltpu.make_async_copy(a, b, local_sem.at[i]) for i, (a, b) in enumerate(loads)]
    for load in loads:
        load.start()

    barrier = pltpu.get_barrier_semaphore()
    for r in range(1, n_sp):
        pl.semaphore_signal(
            barrier, inc=1, device_id={"sp": lax.rem(me + r, n_sp)}, device_id_type=MESH
        )
    for r in range(1, n_dp):
        pl.semaphore_signal(
            barrier, inc=1, device_id={"dp": lax.rem(dp + r, n_dp)}, device_id_type=MESH
        )
    pl.semaphore_wait(barrier, n_sp - 1 + n_dp - 1)
    for load in loads:
        load.wait()

    def ring_copy(way, part, kind, slot, t):
        if kind == 0:
            rows = tok // 2
            ref = x_all.at[slot, part * rows : (part + 1) * rows]
        else:
            rows = wo_all.shape[2] // 2
            ref = wo_all.at[dp, slot, part * rows : (part + 1) * rows]
        return pltpu.make_async_remote_copy(
            src_ref=ref,
            dst_ref=ref,
            send_sem=ring_send.at[way, part, kind, t],
            recv_sem=ring_recv.at[way, part, kind, t],
            device_id={"sp": at_pos(pos + 1 - 2 * way)},
            device_id_type=MESH,
        )

    def slot_at(way, distance):
        return at_pos(pos - (1 - 2 * way) * distance)

    def w_copy(r, source):
        return pltpu.make_async_remote_copy(
            src_ref=w_all.at[source],
            dst_ref=w_all.at[source],
            send_sem=w_send.at[r - 1],
            recv_sem=w_recv.at[r - 1],
            device_id={"dp": lax.rem(dp + r, n_dp)},
            device_id_type=MESH,
        )

    def wo_copy(r, source, slot):
        return pltpu.make_async_remote_copy(
            src_ref=wo_all.at[source, slot],
            dst_ref=wo_all.at[source, slot],
            send_sem=wo_send.at[r - 1, slot],
            recv_sem=wo_recv.at[r - 1, slot],
            device_id={"dp": lax.rem(dp + r, n_dp)},
            device_id_type=MESH,
        )

    def spread(slot):
        for r in range(1, n_dp):
            wo_copy(r, dp, slot).start()

    def project(slot):
        raw = jnp.dot(
            x_all[slot],
            w_all[...].reshape(w_all.shape[0] * w_all.shape[1], w_all.shape[2]),
            preferred_element_type=jnp.float32,
        )
        lanes = lax.broadcasted_iota(jnp.int32, (GRID_W, HD), 1)
        grid_rows = tok // GRID_W

        def table(ref):
            parts = []
            for g in range(grid_rows):
                row = ref[pl.ds(slot * grid_rows + g, 1), :]
                parts.append(
                    jnp.where(lanes < HD // 2, jnp.broadcast_to(row, (GRID_W, HD)), ref[0:GRID_W, :])
                )
            return jnp.concatenate(parts, axis=0)

        cosine = table(cos_ref)
        sine = table(sin_ref)
        even = lax.broadcasted_iota(jnp.int32, (tok, HD), 1) % 2 == 0
        rows = pl.ds(pl.multiple_of(slot * tok, tok), tok)
        for h in range(hq + hk):
            r = raw[:, h * HD : (h + 1) * HD]
            gain = gain_ref[0:1, :] if h < hq else gain_ref[1:2, :]
            n = r * lax.rsqrt(jnp.mean(r * r, axis=-1, keepdims=True) + EPS) * gain
            swapped = jnp.where(even, pltpu.roll(n, HD - 1, 1), pltpu.roll(n, 1, 1))
            turned = (n * cosine + swapped * sine).astype(jnp.bfloat16)
            if h < hq:
                q_s[h, rows, :] = turned
            else:
                k_s[h - hq, rows, :] = turned
        for h in range(hk):
            v_s[h, rows, :] = raw[:, (hq + hk + h) * HD : (hq + hk + h + 1) * HD].astype(
                jnp.bfloat16
            )

    for r in range(1, n_dp):
        w_copy(r, dp).start()
    for part in (0, 1):
        for kind in (0, 1):
            for way in (0, 1):
                ring_copy(way, part, kind, me, 0).start()
    spread(me)
    for r in range(1, n_dp):
        w_copy(r, lax.rem(dp - r + n_dp, n_dp)).wait_recv()
    project(me)

    @pl.loop(1, half)
    def _(t):
        for part in (0, 1):
            for kind in (0, 1):
                for way in (0, 1):
                    slot = slot_at(way, t)
                    ring_copy(way, part, kind, slot, t - 1).wait_recv()
                    if way == part:
                        ring_copy(way, part, kind, slot, t).start()
                    else:

                        @pl.when(t < half - 1)
                        def _():
                            ring_copy(way, part, kind, slot, t).start()

        for way in (0, 1):
            spread(slot_at(way, t))

        @pl.loop(0, 2)
        def _(way):
            project(slot_at(way, t))

    far = at_pos(pos + half)
    for kind in (0, 1):
        for way in (0, 1):
            ring_copy(way, way, kind, far, half - 1).wait_recv()
    spread(far)
    project(far)

    c = HD ** (-0.5) * LOG2E

    def att_copy(slot, source):
        return pltpu.make_async_remote_copy(
            src_ref=att_s.at[slot],
            dst_ref=att_all.at[source],
            send_sem=att_send.at[slot],
            recv_sem=att_recv.at[source],
            device_id={"sp": slot},
            device_id_type=MESH,
        )

    def attend(slot):
        rows = pl.ds(pl.multiple_of(slot * tok, tok), tok)
        for h in range(hq):
            g = h * hk // hq
            s = lax.dot_general(
                q_s[h, rows, :],
                k_s[g],
                (((1,), (1,)), ((), ())),
                preferred_element_type=jnp.float32,
            )
            p = jnp.exp2((s - jnp.max(s, axis=1, keepdims=True)) * c)
            inv = 1.0 / jnp.sum(p, axis=1, keepdims=True)
            probs = (p * inv).astype(jnp.bfloat16)
            att_s[slot, :, h * HD : (h + 1) * HD] = jnp.dot(
                probs, v_s[g], preferred_element_type=jnp.float32
            ).astype(jnp.bfloat16)

    @pl.loop(1, n_sp + 1)
    def _(r):
        slot = lax.rem(me + r, n_sp)
        attend(slot)

        @pl.when(r < n_sp)
        def _():
            att_copy(slot, me).start()

    att_all[me] = att_s[me]

    @pl.loop(1, n_sp)
    def _(r):
        source = lax.rem(me + r, n_sp)
        pltpu.make_async_remote_copy(
            src_ref=att_s.at[source],
            dst_ref=att_all.at[source],
            send_sem=att_send.at[source],
            recv_sem=att_recv.at[source],
            device_id={"sp": source},
            device_id_type=MESH,
        ).wait_recv()

    @pl.loop(0, n_sp)
    def _(slot):
        for r in range(1, n_dp):
            wo_copy(r, lax.rem(dp - r + n_dp, n_dp), slot).wait_recv()

    depth, cols = wo_all.shape[2], wo_all.shape[3]
    feat = hq * HD
    per = depth // feat

    @pl.loop(0, n_sp)
    def _(block):
        total = None
        for s in range(n_sp):
            term = jnp.dot(
                att_all[s],
                wo_all[s // per, block, (s % per) * feat : (s % per + 1) * feat, :],
                preferred_element_type=jnp.float32,
            )
            total = term if total is None else total + term
        out_ref[:, pl.ds(pl.multiple_of(block * cols, cols), cols)] = total.astype(out_ref.dtype)

    for r in range(1, n_dp):
        w_copy(r, dp).wait_send()

    @pl.loop(0, n_sp)
    def _(slot):
        for r in range(1, n_dp):
            wo_copy(r, dp, slot).wait_send()

    @pl.loop(0, half)
    def _(t):
        for part in (0, 1):
            for kind in (0, 1):
                for way in (0, 1):
                    if way == part:
                        ring_copy(way, part, kind, slot_at(way, t), t).wait_send()
                    else:

                        @pl.when(t < half - 1)
                        def _():
                            ring_copy(way, part, kind, slot_at(way, t), t).wait_send()

    @pl.loop(1, n_sp)
    def _(r):
        att_copy(lax.rem(me + r, n_sp), me).wait_send()


def on_device(tokens, w_query, w_key, w_value, w_out, qk_gain):
    n_sp = lax.axis_size("sp")
    n_dp = lax.axis_size("dp")
    own_rows = tokens[0]
    tok, width = own_rows.shape
    seq_len = tok * n_sp
    hq = HQ // n_sp
    hk = max(1, KV // n_sp)
    cosine, sine = rope_tables(seq_len)
    any_spec = pl.BlockSpec(memory_space=pl.ANY)
    vmem_spec = pl.BlockSpec(memory_space=pltpu.VMEM)
    half = n_sp // 2
    dma = pltpu.SemaphoreType.DMA
    bf16 = jnp.bfloat16
    out = pl.pallas_call(
        functools.partial(layer_kernel, n_sp, n_dp, hq, hk),
        out_shape=jax.ShapeDtypeStruct((tok, n_sp * w_out.shape[1]), bf16),
        in_specs=[any_spec] * 5 + [vmem_spec] * 3,
        out_specs=vmem_spec,
        scratch_shapes=[
            pltpu.VMEM((n_sp, tok, width), bf16),
            pltpu.VMEM((n_dp, w_query.shape[0], (hq + 2 * hk) * HD), bf16),
            pltpu.VMEM((n_dp, n_sp) + w_out.shape, bf16),
            pltpu.VMEM((hq, seq_len, HD), bf16),
            pltpu.VMEM((hk, seq_len, HD), bf16),
            pltpu.VMEM((hk, seq_len, HD), bf16),
            pltpu.VMEM((n_sp, tok, hq * HD), bf16),
            pltpu.VMEM((n_sp, tok, hq * HD), bf16),
            dma((5,)),
            dma((2, 2, 2, half)),
            dma((2, 2, 2, half)),
            dma((n_dp - 1,)),
            dma((n_dp - 1,)),
            dma((n_dp - 1, n_sp)),
            dma((n_dp - 1, n_sp)),
            dma((n_sp,)),
            dma((n_sp,)),
        ],
        compiler_params=pltpu.CompilerParams(
            collective_id=0, has_side_effects=True, vmem_limit_bytes=VMEM_CAP
        ),
    )(
        own_rows,
        w_query,
        head_columns(w_key, n_sp),
        head_columns(w_value, n_sp),
        w_out,
        cosine,
        sine,
        qk_gain,
    )
    return out[None]


def head_columns(weight, n_sp):
    local = weight.shape[1]
    if local >= HD:
        return weight
    group = HD // local
    groups = [list(range(g, g + group)) for g in range(0, n_sp, group)]
    return lax.all_gather(weight, "sp", axis=1, tiled=True, axis_index_groups=groups)


def solution(mesh):
    in_specs = (
        P("dp", "sp", None),
        P("dp", "sp"),
        P("dp", "sp"),
        P("dp", "sp"),
        P("dp", "sp"),
        P(),
    )
    return jax.shard_map(
        on_device, mesh=mesh, in_specs=in_specs, out_specs=P("dp", "sp", None), check_vma=False
    )
```

time: 267 us -> 144 us (0.54)
  waiting for transfers between devices: 199 us -> 0 us
  Pallas kernels: 39.7 us -> 140 us
  between operations: 13.2 us -> 0.01 us
  starting transfers between devices: 6.38 us -> 0 us
  other arithmetic: 4.93 us -> 0.92 us
    all_gather x3 -> x0, waiting for transfers between devices: 197 us -> none  [the longest x1 123 us: on_device(): seq_rows = lax.all_gather(own_rows, 'sp', axis=0, tiled=True)]
    pallas_call x2 -> x1, Pallas kernels: 39.7 us -> 140 us  [on_device(): pl.pallas_call(functools.partial(layer_kernel, n_sp, n_dp, hq, hk), out_s...]
    all_to_all x1 -> x0, starting transfers between devices: 6.3 us -> none  [on_device(): lax.all_to_all(attended.reshape(n_sp, tok, hq * HD), 'sp', split_axis=0,...]
    concatenate x3 -> x0, other arithmetic: 4.57 us -> none  [the longest x2 2.62 us: table(): return jnp.concatenate([by_row, by_col], axis=2).reshape(seq_len, HD)]
  transfers between devices with their start and end apart: 4 -> 0, of which waited for: 3 -> 0; matrix products, arithmetic and copies ran while one was open for 1% -> 0% of each run, Pallas kernels for 12% -> 0%
where the time goes in v2:
time: 144 us
  Pallas kernels  140 us (97%)
  local copies, waits for them, and re-layouts  2.49 us (2%)
    pallas_call x1, Pallas kernels, on_device(): pl.pallas_call(functools.partial(layer_kernel, n_sp, n_dp, hq, hk), out_s...  140 us

profile of v2, /device:TPU:13, one launch (start us, length us, event | category | flops | bytes accessed | tf_op | source)
XLA Modules:
  0.0 143.6 jit_solution(3425097511312539437)
XLA Ops:
  0.0 0.1 broadcast_in_dim.19
  0.1 0.1 reshape.21
  0.2 0.1 compare_select_fusion
  0.3 0.8 fusion
  1.1 140.2 %shard_map.64 = bf16[256,2048]{1,0:T(8,128)(2,1)} custom-call(bf16[256,2048]{1,0:T(8,128)(2,1)} %bitcast.3, bf16[512,256]{1,0:T(8,128)(2,1)} %wq_ref.1, bf16[512,128]{1,0:T(8,128)(2,1)} %wk_ref.1, bf16[512,128]{1,0:T(8,128)(2,1)} %wv_ref.1, bf16[512,256]{1,0:T(8,128)(2,1)} %wo_ref.1, f32[64,128]{1,0:T(8,128)} %get-tuple-element.6.cos_ref, ...), custom_call_target="tpu_custom_call" | custom-call | tf_op jit(solution)/shard_map/pallas_call | solution.py:309
  141.3 2.3 %copy.8 = bf16[1,256,2048]{2,1,0:T(8,128)(2,1)} copy(bf16[1,256,2048]{2,1,0:T(8,128)(2,1)} %bitcast.2) | data formatting | bytes 2097152
  (2 shorter events, 0.0 us)

commit v3 on v2

--- a/solution.py
+++ b/solution.py
@@ -155,8 +155,8 @@
 
     for r in range(1, n_dp):
         w_copy(r, dp).start()
-    for part in (0, 1):
-        for kind in (0, 1):
+    for kind in (0, 1):
+        for part in (0, 1):
             for way in (0, 1):
                 ring_copy(way, part, kind, me, 0).start()
     spread(me)
@@ -166,8 +166,8 @@
 
     @pl.loop(1, half)
     def _(t):
-        for part in (0, 1):
-            for kind in (0, 1):
+        for kind in (0, 1):
+            for part in (0, 1):
                 for way in (0, 1):
                     slot = slot_at(way, t)
                     ring_copy(way, part, kind, slot, t - 1).wait_recv()
@@ -187,11 +187,12 @@
             project(slot_at(way, t))
 
     far = at_pos(pos + half)
-    for kind in (0, 1):
-        for way in (0, 1):
-            ring_copy(way, way, kind, far, half - 1).wait_recv()
+    for way in (0, 1):
+        ring_copy(way, way, 0, far, half - 1).wait_recv()
+    project(far)
+    for way in (0, 1):
+        ring_copy(way, way, 1, far, half - 1).wait_recv()
     spread(far)
-    project(far)
 
     c = HD ** (-0.5) * LOG2E
 

time: 144 us -> 143 us (level)
  no operation moved by 1% of the time
where the time goes in v3:
time: 143 us
  Pallas kernels  139 us (97%)
  local copies, waits for them, and re-layouts  2.49 us (2%)
    pallas_call x1, Pallas kernels, on_device(): pl.pallas_call(functools.partial(layer_kernel, n_sp, n_dp, hq, hk), out_s...  139 us

profile of v3, /device:TPU:13, one launch (start us, length us, event | category | flops | bytes accessed | tf_op | source)
XLA Modules:
  0.0 142.6 jit_solution(13438403063817568269)
XLA Ops:
  0.0 0.1 broadcast_in_dim.19
  0.1 0.1 reshape.21
  0.2 0.1 compare_select_fusion
  0.3 0.8 fusion
  1.1 139.2 %shard_map.64 = bf16[256,2048]{1,0:T(8,128)(2,1)} custom-call(bf16[256,2048]{1,0:T(8,128)(2,1)} %bitcast.3, bf16[512,256]{1,0:T(8,128)(2,1)} %wq_ref.1, bf16[512,128]{1,0:T(8,128)(2,1)} %wk_ref.1, bf16[512,128]{1,0:T(8,128)(2,1)} %wv_ref.1, bf16[512,256]{1,0:T(8,128)(2,1)} %wo_ref.1, f32[64,128]{1,0:T(8,128)} %get-tuple-element.6.cos_ref, ...), custom_call_target="tpu_custom_call" | custom-call | tf_op jit(solution)/shard_map/pallas_call | solution.py:310
  140.3 2.3 %copy.8 = bf16[1,256,2048]{2,1,0:T(8,128)(2,1)} copy(bf16[1,256,2048]{2,1,0:T(8,128)(2,1)} %bitcast.2) | data formatting | bytes 2097152
  (2 shorter events, 0.0 us)
